TPU v7x, 32 devices: a whole 2x2x4 slice. The times are simulated.
32 devices in a mesh: rep: 2 (over x), fs: 8 (over z, y), tp: 2 (over core).
Axes of the slice: x: 2, y: 2, z: 4, core: 2. Of those that a mesh axis runs over, the one named last changes fastest.
Arguments:
- block_input: bfloat16 [8192, 2048], P(('rep', 'fs', 'tp')), may hold values from -6 to 6
- pre_gain: float32 [2048], replicated, may hold values from 0.1 to 1.9
- post_gain: float32 [2048], replicated, may hold values from 0.1 to 1.9
- gate_saved: bfloat16 [8192, 5632], P(('rep', 'fs'), 'tp'), may hold values from -8 to 8
- up_saved: bfloat16 [8192, 5632], P(('rep', 'fs'), 'tp'), may hold values from -6 to 6
- branch_saved: bfloat16 [8192, 2048], P(('rep', 'fs', 'tp')), may hold values from -6 to 6
- out_cotangent: bfloat16 [8192, 2048], P(('rep', 'fs', 'tp')), may hold values from -6 to 6
- gate_weight: bfloat16 [2048, 5632], P('fs', 'tp'), may hold values from -0.125 to 0.125
- up_weight: bfloat16 [2048, 5632], P('fs', 'tp'), may hold values from -0.125 to 0.125
- down_weight: bfloat16 [2048, 5632], P('fs', 'tp'), may hold values from -0.078125 to 0.078125
Outputs:
- input_grad: bfloat16 [8192, 2048], P(('rep', 'fs', 'tp'))
- gate_grad: float32 [2048, 5632], P('fs', 'tp')
- up_grad: float32 [2048, 5632], P('fs', 'tp')
- down_grad: float32 [2048, 5632], P('fs', 'tp')
All inputs are finite; a program needn't handle non-finite values.
Results may differ from a plain program's by a relative error of at most 0.018.
Values may be sent and summed in bfloat16 or wider, within the bound.
A program may use at most 128 MiB of HBM per device.

v0:
```python
import jax
import jax.numpy as jnp
from jax import lax
from jax.sharding import PartitionSpec as P

eps = 1e-06


def contract_rows(left, right):
    return lax.dot_general(
        left, right, (((0,), (0,)), ((), ())), preferred_element_type=jnp.float32
    )


def contract_cols(left, right):
    return lax.dot_general(
        left, right, (((1,), (1,)), ((), ())), preferred_element_type=jnp.float32
    )


def per_device(
    block_input,
    pre_gain,
    post_gain,
    gate_saved,
    up_saved,
    branch_saved,
    out_cotangent,
    gate_weight,
    up_weight,
    down_weight,
):
    xfull = block_input.astype(jnp.float32)
    inv_x = lax.rsqrt(jnp.mean(xfull * xfull, axis=-1, keepdims=True) + eps)
    normed = (xfull * inv_x * pre_gain).astype(jnp.bfloat16)
    branch = branch_saved.astype(jnp.float32)
    inv_b = lax.rsqrt(jnp.mean(branch * branch, axis=-1, keepdims=True) + eps)
    upstream = 0.5 * out_cotangent.astype(jnp.float32) * post_gain
    branch_grad = (
        inv_b * upstream - branch * inv_b**3 * jnp.mean(upstream * branch, axis=-1, keepdims=True)
    ).astype(jnp.bfloat16)
    gate_full, up_full, down_full = (
        lax.all_gather(gate_weight, "fs", axis=0, tiled=True),
        lax.all_gather(up_weight, "fs", axis=0, tiled=True),
        lax.all_gather(down_weight, "fs", axis=0, tiled=True),
    )
    normed_rows, branch_rows = (
        lax.all_gather(normed, "tp", axis=0, tiled=True),
        lax.all_gather(branch_grad, "tp", axis=0, tiled=True),
    )
    gate_f = gate_saved.astype(jnp.float32)
    up_f = up_saved.astype(jnp.float32)
    sigma = jax.nn.sigmoid(gate_f)
    silu_gate = gate_f * sigma
    hidden = (silu_gate * up_f).astype(jnp.bfloat16)
    hidden_grad = jnp.dot(branch_rows, down_full, preferred_element_type=jnp.float32)
    gate_cot = (hidden_grad * up_f * sigma * (1.0 + gate_f * (1.0 - sigma))).astype(jnp.bfloat16)
    up_cot = (hidden_grad * silu_gate).astype(jnp.bfloat16)
    normed_grad = lax.psum_scatter(
        (contract_cols(gate_cot, gate_full) + contract_cols(up_cot, up_full)).astype(jnp.bfloat16),
        "tp",
        scatter_dimension=0,
        tiled=True,
    ).astype(jnp.float32)
    scaled = normed_grad * pre_gain
    input_grad = (
        out_cotangent.astype(jnp.float32)
        + inv_x * scaled
        - xfull * inv_x**3 * jnp.mean(scaled * xfull, axis=-1, keepdims=True)
    )
    gate_sum = contract_rows(normed_rows, gate_cot)
    up_sum = contract_rows(normed_rows, up_cot)
    down_sum = contract_rows(branch_rows, hidden)
    shards = (
        lax.psum_scatter(
            gate_sum.astype(jnp.bfloat16), "fs", scatter_dimension=0, tiled=True
        ).astype(jnp.float32),
        lax.psum_scatter(up_sum.astype(jnp.bfloat16), "fs", scatter_dimension=0, tiled=True).astype(
            jnp.float32
        ),
        lax.psum_scatter(
            down_sum.astype(jnp.bfloat16), "fs", scatter_dimension=0, tiled=True
        ).astype(jnp.float32),
    )
    gate_grad, up_grad, down_grad = (
        lax.psum(shards[0].astype(jnp.bfloat16), "rep").astype(jnp.float32),
        lax.psum(shards[1].astype(jnp.bfloat16), "rep").astype(jnp.float32),
        lax.psum(shards[2].astype(jnp.bfloat16), "rep").astype(jnp.float32),
    )
    return (input_grad.astype(jnp.bfloat16), gate_grad, up_grad, down_grad)


def solution(mesh):
    return jax.shard_map(
        per_device,
        mesh=mesh,
        in_specs=(
            P(("rep", "fs", "tp"), None),
            P(),
            P(),
            P(("rep", "fs"), "tp"),
            P(("rep", "fs"), "tp"),
            P(("rep", "fs", "tp"), None),
            P(("rep", "fs", "tp"), None),
            P("fs", "tp"),
            P("fs", "tp"),
            P("fs", "tp"),
        ),
        out_specs=(P(("rep", "fs", "tp"), None), P("fs", "tp"), P("fs", "tp"), P("fs", "tp")),
        check_vma=False,
    )
```

profile of v0, /device:TPU:0, one launch (start us, length us, event | category | flops | bytes accessed | tf_op | source)
XLA Modules:
  0.0 1274.3 jit_solution(7613329253536069101)
XLA Ops:
  7.2 0.0 all-gather.6.cloned.1.call-start
  7.2 0.7 broadcast_multiply_fusion
  7.9 2.1 fusion.14
  10.0 3.1 fusion.11
  13.1 0.0 copy-start.5
  13.1 0.0 all-gather.6.cloned.1.call-update
  13.1 0.0 all-gather.8.cloned.1.call-start
  13.2 0.7 all-gather.8.cloned.1.call-update
  13.9 0.0 all-gather.10.cloned.1.call-start
  13.9 0.7 all-gather.10.cloned.1.call-update
  14.6 0.0 all-gather.12.cloned.1.call-start
  14.7 0.5 all-gather.12.cloned.1.call-update
  15.2 0.0 reduce-scatter.5.cloned.1.call-start
  15.2 11.3 all-gather.6.cloned.1.call-done
  26.6 166.7 %all-gather.8.cloned.1.call-done = bf16[2048,2816]{1,0:T(8,128)(2,1)} async-done(((bf16[256,2816]{1,0:T(8,128)(2,1)}), bf16[2048,2816]{1,0:T(8,128)(2,1)}) %all-gather.8.cloned.1.call-update) | async-done | bytes 11534352 | tf_op jit(solution)/shard_map/all_gather | solution.py:45
  193.3 0.0 copy-done.5
  193.3 14.0 %fusion.2 = (bf16[512,2816]{1,0:T(8,128)(2,1)}, f32[512,2816]{1,0:T(8,128)}) fusion(bf16[512,2816]{1,0:T(8,128)(2,1)S(1)} %copy-done.5, bf16[512,2816]{1,0:T(8,128)(2,1)} %param.13, bf16[512,2048]{1,0:T(8,128)(2,1)} %all-gather.6.cloned.1.call-done, bf16[2048,2816]{1,0:T(8,128)(2,1)} %all-gather.8.cloned.1.call-done), kind=kOutput, calls=%fused_computation.10 | convolution fusion | flops 5922881536 | bytes 28049408 | tf_op jit(solution)/shard_map/dot_general | solution.py:56
  207.3 149.7 %all-gather.10.cloned.1.call-done = bf16[2048,2816]{1,0:T(8,128)(2,1)} async-done(((bf16[256,2816]{1,0:T(8,128)(2,1)}), bf16[2048,2816]{1,0:T(8,128)(2,1)}) %all-gather.10.cloned.1.call-update) | async-done | bytes 11534352 | tf_op jit(solution)/shard_map/all_gather | solution.py:43
  357.0 11.2 fusion.23
  368.2 152.3 %all-gather.12.cloned.1.call-done = bf16[2048,2816]{1,0:T(8,128)(2,1)} async-done(((bf16[256,2816]{1,0:T(8,128)(2,1)}), bf16[2048,2816]{1,0:T(8,128)(2,1)}) %all-gather.12.cloned.1.call-update) | async-done | bytes 11534352 | tf_op jit(solution)/shard_map/all_gather | solution.py:44
  520.6 0.0 copy-start.1
  520.6 0.0 copy-start.4
  520.6 13.4 %add_convert_fusion = bf16[512,2048]{1,0:T(8,128)(2,1)} fusion(f32[512,2048]{1,0:T(8,128)} %fusion.23, bf16[2048,2816]{1,0:T(8,128)(2,1)} %all-gather.12.cloned.1.call-done, f32[512,2816]{1,0:T(8,128)} %get-tuple-element.18, bf16[512,2816]{1,0:T(8,128)(2,1)} %param.13), kind=kOutput, calls=%fused_computation.17 | convolution fusion | flops 5917769728 | bytes 26476544 | tf_op jit(solution)/shard_map/dot_general | solution.py:16
  534.0 0.0 copy-start
  534.0 0.0 reduce-scatter.5.cloned.1.call-update
  534.0 0.0 all-gather.14.cloned.1.call-start
  534.0 8.0 reduce-scatter.5.cloned.1.call-done
  542.1 0.0 copy-done.1
  542.1 0.0 copy-done.4
  542.1 1.8 fusion.17
  543.9 0.0 copy-done
  543.9 3.5 fusion.21
  547.4 0.0 all-gather.14.cloned.1.call-update
  547.4 0.2 reduce-scatter.11.cloned.1.call-start
  547.6 12.3 convolution_convert_fusion
  559.9 0.0 copy-start.6
  559.9 0.0 reduce-scatter.11.cloned.1.call-update
  559.9 0.0 reduce-scatter.9.cloned.1.call-start
  560.0 0.0 all-gather.14.cloned.1.call-done
  560.0 1.7 copy-done.6
  561.7 12.2 convolution_convert_fusion.1
  573.9 0.0 copy-start.7
  573.9 0.0 reduce-scatter.9.cloned.1.call-update
  573.9 0.0 reduce-scatter.7.cloned.1.call-start
  574.0 1.5 copy-done.7
  575.5 10.7 convolution_convert_fusion.2
  586.2 0.0 reduce-scatter.7.cloned.1.call-update
  586.2 0.0 all-reduce.3.cloned.1.call-start
  586.3 170.7 %reduce-scatter.11.cloned.1.call-done = bf16[256,2816]{1,0:T(8,128)(2,1)} async-done(((bf16[2048,2816]{1,0:T(8,128)(2,1)}), bf16[256,2816]{1,0:T(8,128)(2,1)}) %reduce-scatter.11.cloned.1.call-update) | async-done | bytes 1441808 | tf_op jit(solution)/shard_map/reduce_scatter | solution.py:81
  757.0 195.6 %reduce-scatter.9.cloned.1.call-done = bf16[256,2816]{1,0:T(8,128)(2,1)} async-done(((bf16[2048,2816]{1,0:T(8,128)(2,1)}), bf16[256,2816]{1,0:T(8,128)(2,1)}) %reduce-scatter.9.cloned.1.call-update) | async-done | bytes 1441808 | tf_op jit(solution)/shard_map/reduce_scatter | solution.py:78
  952.6 195.5 %reduce-scatter.7.cloned.1.call-done = bf16[256,2816]{1,0:T(8,128)(2,1)} async-done(((bf16[2048,2816]{1,0:T(8,128)(2,1)}), bf16[256,2816]{1,0:T(8,128)(2,1)}) %reduce-scatter.7.cloned.1.call-update) | async-done | bytes 1441808 | tf_op jit(solution)/shard_map/reduce_scatter | solution.py:75
  1148.2 0.0 all-reduce.3.cloned.1.call-update
  1148.2 112.4 %all-reduce.3.cloned.1.call-done = (bf16[256,2816]{1,0:T(8,128)(2,1)}, bf16[256,2816]{1,0:T(8,128)(2,1)}, bf16[256,2816]{1,0:T(8,128)(2,1)}) async-done(((bf16[256,2816]{1,0:T(8,128)(2,1)}, bf16[256,2816]{1,0:T(8,128)(2,1)}, bf16[256,2816]{1,0:T(8,128)(2,1)}), (bf16[256,2816]{1,0:T(8,128)(2,1)}, bf16[256,2816]{1,0:T(8,128)(2,1)}, bf16[256,2816]{1,0:T(8,128)(2,1)})) %all-reduce.3.cloned.1.call-update) | async-done | bytes 4325392 | tf_op jit(solution)/shard_map/psum | solution.py:86
  1260.5 0.0 copy-start.3
  1260.5 3.2 convert_element_type.77
  1263.8 0.0 copy-start.2
  1263.8 0.0 copy-done.3
  1263.8 1.8 convert_element_type.79
  1265.6 0.2 copy-done.2
  1265.7 1.8 convert_element_type.82
  (3 shorter events, 0.0 us)
Async XLA Ops:
  7.2 19.4 %all-gather.6.cloned.1.call-start = ((), (), s32[]{:S(2)}) async-start(), calls=%async_computation.4 | async-start | bytes 3145728 | tf_op jit(solution)/shard_map/all_gather | solution.py:49
  13.1 180.2 %copy-start.5 = (bf16[512,2816]{1,0:T(8,128)(2,1)S(1)}, bf16[512,2816]{1,0:T(8,128)(2,1)}, u32[]{:S(2)}) copy-start(bf16[512,2816]{1,0:T(8,128)(2,1)} %param.14) | copy-start | bytes 8650756
  13.1 180.2 %all-gather.8.cloned.1.call-start = ((), (), s32[]{:S(2)}) async-start(), calls=%async_computation.5 | async-start | bytes 12976128 | tf_op jit(solution)/shard_map/all_gather | solution.py:45
  13.9 343.1 %all-gather.10.cloned.1.call-start = ((), (), s32[]{:S(2)}) async-start(), calls=%async_computation.6 | async-start | bytes 12976128 | tf_op jit(solution)/shard_map/all_gather | solution.py:43
  14.6 506.0 %all-gather.12.cloned.1.call-start = ((), (), s32[]{:S(2)}) async-start(), calls=%async_computation.7 | async-start | bytes 12976128 | tf_op jit(solution)/shard_map/all_gather | solution.py:44
  15.2 526.9 %reduce-scatter.5.cloned.1.call-start = ((), (), s32[]{:S(2)}) async-start(), calls=%async_computation.8 | async-start | bytes 3145728 | tf_op jit(solution)/shard_map/reduce_scatter | solution.py:59
  520.6 21.5 %copy-start.1 = (bf16[256,2048]{1,0:T(8,128)(2,1)S(1)}, bf16[256,2048]{1,0:T(8,128)(2,1)}, u32[]{:S(2)}) copy-start(bf16[256,2048]{1,0:T(8,128)(2,1)} %param.10) | copy-start | bytes 3145732
  520.6 21.5 %copy-start.4 = (f32[2048]{0:T(1024)S(1)}, f32[2048]{0:T(1024)}, u32[]{:S(2)}) copy-start(f32[2048]{0:T(1024)} %param.11) | copy-start | bytes 24580
  534.0 9.9 copy-start
  534.0 26.0 %all-gather.14.cloned.1.call-start = ((), (), s32[]{:S(2)}) async-start(), calls=%async_computation.9 | async-start | bytes 3145728 | tf_op jit(solution)/shard_map/all_gather | solution.py:48
  547.4 209.6 %reduce-scatter.11.cloned.1.call-start = ((), (), s32[]{:S(2)}) async-start(), calls=%async_computation.12 | async-start | bytes 12976128 | tf_op jit(solution)/shard_map/reduce_scatter | solution.py:81
  559.9 1.8 copy-start.6
  559.9 392.7 %reduce-scatter.9.cloned.1.call-start = ((), (), s32[]{:S(2)}) async-start(), calls=%async_computation.11 | async-start | bytes 12976128 | tf_op jit(solution)/shard_map/reduce_scatter | solution.py:78
  573.9 1.6 copy-start.7
  573.9 574.2 %reduce-scatter.7.cloned.1.call-start = ((), (), s32[]{:S(2)}) async-start(), calls=%async_computation.10 | async-start | bytes 12976128 | tf_op jit(solution)/shard_map/reduce_scatter | solution.py:75
  586.2 674.3 %all-reduce.3.cloned.1.call-start = ((), (), s32[]{:S(2)}) async-start(), calls=%async_computation.13 | async-start | bytes 8650752 | tf_op jit(solution)/shard_map/psum | solution.py:86
  1260.5 3.2 copy-start.3
  1263.8 1.9 copy-start.2
Sparse Core Ops, SparseCore 0:
  13.3 13.2 all-gather.5
  28.8 164.4 all-gather.7
  195.5 161.4 all-gather.9
  359.1 161.4 all-gather.11
  534.1 7.9 reduce-scatter.4
  547.5 11.8 all-gather.13
  563.0 193.9 reduce-scatter.10
  760.6 191.9 reduce-scatter.8
  956.2 191.8 reduce-scatter.6
  1150.6 109.8 all-reduce.2
where the time goes:
time: 1270 us
  waiting for transfers between devices  1160 us (91%)
  matrix products  73.8 us (6%)
  other arithmetic  17.9 us (1%)
  between operations  14.2 us (1%)
    reduce_scatter x1, waiting for transfers between devices, per_device(): lax.psum_scatter(up_sum.astype(jnp.bfloat16), 'fs', scatter_dimension=0,...  196 us
    reduce_scatter x1, waiting for transfers between devices, per_device(): lax.psum_scatter(gate_sum.astype(jnp.bfloat16), 'fs', scatter_dimension=0...  196 us
    reduce_scatter x1, waiting for transfers between devices, per_device(): lax.psum_scatter(down_sum.astype(jnp.bfloat16), 'fs', scatter_dimension=0...  171 us
    all_gather x1, waiting for transfers between devices, per_device(): lax.all_gather(down_weight, 'fs', axis=0, tiled=True)  167 us
    all_gather x1, waiting for transfers between devices, per_device(): lax.all_gather(up_weight, 'fs', axis=0, tiled=True)  152 us
    all_gather x1, waiting for transfers between devices, per_device(): lax.all_gather(gate_weight, 'fs', axis=0, tiled=True)  150 us
    psum x1, waiting for transfers between devices, per_device(): lax.psum(shards[0].astype(jnp.bfloat16), 'rep').astype(jnp.float32)  112 us
    dot_general x3, matrix products, contract_rows(): lax.dot_general(left, right, (((0,), (0,)), ((), ())), preferred_element_...  35.2 us
  transfers between devices with their start and end apart: 10, of which 9 were waited for; matrix products, arithmetic and copies ran while one was open for 5% of the time, Pallas kernels for 0%

commit v1 on v0

v1 whole, which is shorter than its diff:
```python
import functools

import jax
import jax.numpy as jnp
from jax import lax
from jax.sharding import PartitionSpec as P

eps = 1e-06


def contract_rows(left, right):
    return lax.dot_general(
        left, right, (((0,), (0,)), ((), ())), preferred_element_type=jnp.float32
    )


def contract_cols(left, right):
    return lax.dot_general(
        left, right, (((1,), (1,)), ((), ())), preferred_element_type=jnp.float32
    )


def shifted(value, reps, step):
    return lax.ppermute(value, "rep", [(i, (i + step) % reps) for i in range(reps)])


def per_device(
    reps,
    block_input,
    pre_gain,
    post_gain,
    gate_saved,
    up_saved,
    branch_saved,
    out_cotangent,
    gate_weight,
    up_weight,
    down_weight,
):
    bf16, f32 = jnp.bfloat16, jnp.float32
    me = lax.axis_index("rep")
    width = gate_saved.shape[1] // reps

    def columns(value, owner):
        return lax.dynamic_slice_in_dim(value, owner * width, width, axis=1)

    down_full = lax.all_gather(columns(down_weight, me), "fs", axis=0, tiled=True)

    gates = [columns(gate_saved, me)]
    ups = [columns(up_saved, me)]
    for k in range(1, reps):
        there = lax.rem(me + k, reps)
        gates.append(shifted(columns(gate_saved, there), reps, k))
        ups.append(shifted(columns(up_saved, there), reps, k))

    xfull = block_input.astype(f32)
    inv_x = lax.rsqrt(jnp.mean(xfull * xfull, axis=-1, keepdims=True) + eps)
    normed = (xfull * inv_x * pre_gain).astype(bf16)
    branch = branch_saved.astype(f32)
    inv_b = lax.rsqrt(jnp.mean(branch * branch, axis=-1, keepdims=True) + eps)
    upstream = 0.5 * out_cotangent.astype(f32) * post_gain
    branch_grad = (
        inv_b * upstream - branch * inv_b**3 * jnp.mean(upstream * branch, axis=-1, keepdims=True)
    ).astype(bf16)

    normed_own = [normed] + [shifted(normed, reps, k) for k in range(1, reps)]
    branch_own = [branch_grad] + [shifted(branch_grad, reps, k) for k in range(1, reps)]
    normed_rows = [lax.all_gather(v, "tp", axis=0, tiled=True) for v in normed_own]
    branch_rows = [lax.all_gather(v, "tp", axis=0, tiled=True) for v in branch_own]
    normed_all = jnp.concatenate(normed_rows, axis=0)
    branch_all = jnp.concatenate(branch_rows, axis=0)

    gate_f = jnp.concatenate(gates, axis=0).astype(f32)
    up_f = jnp.concatenate(ups, axis=0).astype(f32)
    sigma = jax.nn.sigmoid(gate_f)
    silu_gate = gate_f * sigma
    hidden = (silu_gate * up_f).astype(bf16)

    def spread(total):
        shard = lax.psum_scatter(total.astype(bf16), "fs", scatter_dimension=0, tiled=True)
        out = jnp.zeros((shard.shape[0], width * reps), f32)
        out = lax.dynamic_update_slice_in_dim(out, shard.astype(f32), me * width, axis=1)
        for k in range(1, reps):
            other = shifted(shard, reps, k).astype(f32)
            out = lax.dynamic_update_slice_in_dim(
                out, other, lax.rem(me - k + reps, reps) * width, axis=1
            )
        return out

    down_grad = spread(contract_rows(branch_all, hidden))

    hidden_grad = jnp.dot(branch_all, down_full, preferred_element_type=f32)
    gate_cot = (hidden_grad * up_f * sigma * (1.0 + gate_f * (1.0 - sigma))).astype(bf16)
    up_cot = (hidden_grad * silu_gate).astype(bf16)
    gate_grad = spread(contract_rows(normed_all, gate_cot))
    up_grad = spread(contract_rows(normed_all, up_cot))

    gate_full = lax.all_gather(columns(gate_weight, me), "fs", axis=0, tiled=True)
    up_full = lax.all_gather(columns(up_weight, me), "fs", axis=0, tiled=True)
    partial = (contract_cols(gate_cot, gate_full) + contract_cols(up_cot, up_full)).astype(bf16)
    rows = partial.shape[0] // reps
    normed_grad = None
    for k in range(reps):
        piece = lax.psum_scatter(
            partial[k * rows : (k + 1) * rows], "tp", scatter_dimension=0, tiled=True
        )
        if k:
            piece = shifted(piece, reps, reps - k)
        piece = piece.astype(f32)
        normed_grad = piece if normed_grad is None else normed_grad + piece

    scaled = normed_grad * pre_gain
    input_grad = (
        out_cotangent.astype(f32)
        + inv_x * scaled
        - xfull * inv_x**3 * jnp.mean(scaled * xfull, axis=-1, keepdims=True)
    )
    return (input_grad.astype(bf16), gate_grad, up_grad, down_grad)


def solution(mesh):
    return jax.shard_map(
        functools.partial(per_device, mesh.shape["rep"]),
        mesh=mesh,
        in_specs=(
            P(("rep", "fs", "tp"), None),
            P(),
            P(),
            P(("rep", "fs"), "tp"),
            P(("rep", "fs"), "tp"),
            P(("rep", "fs", "tp"), None),
            P(("rep", "fs", "tp"), None),
            P("fs", "tp"),
            P("fs", "tp"),
            P("fs", "tp"),
        ),
        out_specs=(P(("rep", "fs", "tp"), None), P("fs", "tp"), P("fs", "tp"), P("fs", "tp")),
        check_vma=False,
    )
```

time: 1270 us -> 791 us (0.62)
  waiting for transfers between devices: 1160 us -> 642 us
  local copies, waits for them, and re-layouts: 3.41 us -> 32.7 us
  starting transfers between devices: 0.58 us -> 14.9 us
    all_gather x5 -> x7, waiting for transfers between devices: 480 us -> 195 us  [the longest x1 80.9 us: per_device(): lax.all_gather(columns(gate_weight, me), 'fs', axis=0, tiled=True)]
    reduce_scatter x4 -> x5, waiting for transfers between devices: 570 us -> 308 us  [the longest x3 289 us: spread(): lax.psum_scatter(total.astype(bf16), 'fs', scatter_dimension=0, tiled=True)]
    ppermute x0 -> x8, waiting for transfers between devices: none -> 139 us  [shifted(): lax.ppermute(value, 'rep', [(i, (i + step) % reps) for i in range(reps)])]
    psum x1 -> x0, waiting for transfers between devices: 112 us -> none  [per_device(): lax.psum(shards[0].astype(jnp.bfloat16), 'rep').astype(jnp.float32)]
    ppermute x0 -> x8, starting transfers between devices: none -> 14 us  [shifted(): lax.ppermute(value, 'rep', [(i, (i + step) % reps) for i in range(reps)])]
  transfers between devices with their start and end apart: 10 -> 20, of which waited for: 9 -> 15; matrix products, arithmetic and copies ran while one was open for 5% -> 11% of each run, Pallas kernels for 0% -> 0%
where the time goes in v1:
time: 791 us
  waiting for transfers between devices  642 us (81%)
  matrix products  71.2 us (9%)
  local copies, waits for them, and re-layouts  32.7 us (4%)
  other arithmetic  15.3 us (2%)
  starting transfers between devices  14.9 us (2%)
  between operations  14.4 us (2%)
    reduce_scatter x3, waiting for transfers between devices, spread(): lax.psum_scatter(total.astype(bf16), 'fs', scatter_dimension=0, tiled=True)  289 us
    ppermute x8, waiting for transfers between devices, shifted(): lax.ppermute(value, 'rep', [(i, (i + step) % reps) for i in range(reps)])  139 us
    all_gather x1, waiting for transfers between devices, per_device(): lax.all_gather(columns(gate_weight, me), 'fs', axis=0, tiled=True)  80.9 us
    all_gather x1, waiting for transfers between devices, per_device(): up_full = lax.all_gather(columns(up_weight, me), 'fs', axis=0, tiled=True)  77.7 us
    all_gather x1, waiting for transfers between devices, per_device(): lax.all_gather(columns(down_weight, me), 'fs', axis=0, tiled=True)  36.6 us
    dot_general x3, matrix products, contract_rows(): lax.dot_general(left, right, (((0,), (0,)), ((), ())), preferred_element_...  33.9 us
    dot_general x2, matrix products, contract_cols(): lax.dot_general(left, right, (((1,), (1,)), ((), ())), preferred_element_...  22.4 us
    reduce_scatter x2, waiting for transfers between devices, per_device(): lax.psum_scatter(partial[k * rows:(k + 1) * rows], 'tp', scatter_dimensio...  19.1 us
  transfers between devices with their start and end apart: 20, of which 15 were waited for; matrix products, arithmetic and copies ran while one was open for 11% of the time, Pallas kernels for 0%

profile of v1, /device:TPU:0, one launch (start us, length us, event | category | flops | bytes accessed | tf_op | source)
XLA Modules:
  0.0 791.0 jit_solution(12480412477546345069)
XLA Ops:
  7.2 0.8 broadcast_multiply_fusion
  8.0 2.1 fusion.14
  10.2 3.1 fusion.11
  13.3 3.0 collective-permute-start
  16.3 23.4 %collective-permute-done = bf16[256,2048]{1,0:T(8,128)(2,1)S(1)} collective-permute-done((bf16[256,2048]{1,0:T(8,128)(2,1)}, bf16[256,2048]{1,0:T(8,128)(2,1)S(1)}, u32[]{:S(2)}, u32[]{:S(2)}) %collective-permute-start) | collective-permute-done | bytes 1048608 | tf_op jit(solution)/shard_map/ppermute | solution.py:24
  39.7 1.0 copy-done.10
  40.8 0.9 constant_dynamic-slice_fusion.6
  41.7 0.0 all-gather.16.cloned.1.call-start
  41.8 2.2 constant_dynamic-slice_fusion
  44.0 0.0 all-gather.14.cloned.1.call-start
  44.1 2.1 constant_dynamic-slice_fusion.1
  46.1 0.0 reduce-scatter.8.cloned.1.call-start
  46.2 1.8 constant_dynamic-slice_fusion.3
  48.0 1.9 collective-permute-start.2
  49.9 1.3 constant_dynamic-slice_fusion.5
  51.3 1.1 collective-permute-start.1
  52.3 3.2 constant_dynamic-update-slice_fusion.1
  55.5 3.3 constant_dynamic-update-slice_fusion
  58.8 24.0 %collective-permute-done.2 = bf16[512,1408]{1,0:T(8,128)(2,1)} collective-permute-done((bf16[512,1408]{1,0:T(8,128)(2,1)}, bf16[512,1408]{1,0:T(8,128)(2,1)}, u32[]{:S(2)}, u32[]{:S(2)}) %collective-permute-start.2) | collective-permute-done | bytes 1441824 | tf_op jit(solution)/shard_map/ppermute | solution.py:24
  82.8 29.2 %collective-permute-done.1 = bf16[512,1408]{1,0:T(8,128)(2,1)} collective-permute-done((bf16[512,1408]{1,0:T(8,128)(2,1)}, bf16[512,1408]{1,0:T(8,128)(2,1)}, u32[]{:S(2)}, u32[]{:S(2)}) %collective-permute-start.1) | collective-permute-done | bytes 1441824 | tf_op jit(solution)/shard_map/ppermute | solution.py:24
  112.0 36.6 %all-gather.12.cloned.1.call-done = bf16[2048,1408]{1,0:T(8,128)(2,1)} async-done(((bf16[256,1408]{1,0:T(8,128)(2,1)}), bf16[2048,1408]{1,0:T(8,128)(2,1)}) %all-gather.12.cloned.1.call-update) | async-done | bytes 5767184 | tf_op jit(solution)/shard_map/all_gather | solution.py:47
  148.6 14.9 %fusion.2 = (bf16[1024,1408]{1,0:T(8,128)(2,1)}, bf16[1024,1408]{1,0:T(8,128)(2,1)}) fusion(bf16[512,1408]{1,0:T(8,128)(2,1)} %collective-permute-done.1, bf16[512,1408]{1,0:T(8,128)(2,1)S(1)} %get-tuple-element.12, bf16[512,1408]{1,0:T(8,128)(2,1)} %collective-permute-done.2, bf16[512,1408]{1,0:T(8,128)(2,1)S(1)} %copy-done.8, ...), kind=kOutput, calls=%fused_computation.11 | convolution fusion | flops 5935857664 | bytes 21495808 | tf_op jit(solution)/shard_map/dot_general | solution.py:92
  163.5 77.7 %all-gather.16.cloned.1.call-done = bf16[2048,1408]{1,0:T(8,128)(2,1)} async-done(((bf16[256,1408]{1,0:T(8,128)(2,1)}), bf16[2048,1408]{1,0:T(8,128)(2,1)}) %all-gather.16.cloned.1.call-update) | async-done | bytes 5767184 | tf_op jit(solution)/shard_map/all_gather | solution.py:99
  241.2 11.7 %fusion.25 = f32[1024,2048]{1,0:T(8,128)} fusion(bf16[1024,1408]{1,0:T(8,128)(2,1)} %get-tuple-element.9, bf16[2048,1408]{1,0:T(8,128)(2,1)} %all-gather.16.cloned.1.call-done), kind=kOutput, calls=%fused_computation.70 | convolution fusion | flops 5905580032 | bytes 17039360 | tf_op jit(solution)/shard_map/dot_general | solution.py:18
  252.9 80.9 %all-gather.14.cloned.1.call-done = bf16[2048,1408]{1,0:T(8,128)(2,1)} async-done(((bf16[256,1408]{1,0:T(8,128)(2,1)}), bf16[2048,1408]{1,0:T(8,128)(2,1)}) %all-gather.14.cloned.1.call-update) | async-done | bytes 5767184 | tf_op jit(solution)/shard_map/all_gather | solution.py:98
  333.8 10.7 %add_convert_fusion = bf16[1024,2048]{1,0:T(8,128)(2,1)S(1)} fusion(f32[1024,2048]{1,0:T(8,128)} %fusion.25, bf16[1024,1408]{1,0:T(8,128)(2,1)S(1)} %copy-done.17, bf16[2048,1408]{1,0:T(8,128)(2,1)} %all-gather.14.cloned.1.call-done), kind=kOutput, calls=%fused_computation.3 | convolution fusion | flops 5909774336 | bytes 21233664 | tf_op jit(solution)/shard_map/dot_general | solution.py:18
  344.5 2.6 fusion.24
  347.1 0.7 reduce-scatter.6.cloned.1.call-update
  347.8 0.2 all-gather.18.cloned.1.call-start
  348.1 7.1 reduce-scatter.8.cloned.1.call-done
  355.2 1.8 collective-permute-start.3
  357.0 12.0 %reduce-scatter.6.cloned.1.call-done = bf16[256,2048]{1,0:T(8,128)(2,1)} async-done(((bf16[512,2048]{1,0:T(8,128)(2,1)}), bf16[256,2048]{1,0:T(8,128)(2,1)}) %reduce-scatter.6.cloned.1.call-update) | async-done | bytes 1048592 | tf_op jit(solution)/shard_map/reduce_scatter | solution.py:104
  369.0 11.7 %collective-permute-done.3 = bf16[256,2048]{1,0:T(8,128)(2,1)S(1)} collective-permute-done((bf16[256,2048]{1,0:T(8,128)(2,1)}, bf16[256,2048]{1,0:T(8,128)(2,1)S(1)}, u32[]{:S(2)}, u32[]{:S(2)}) %collective-permute-start.3) | collective-permute-done | bytes 1048608 | tf_op jit(solution)/shard_map/ppermute | solution.py:24
  380.8 1.9 fusion.17
  382.7 2.3 fusion.21
  385.2 1.7 collective-permute-start.4
  386.9 23.1 %collective-permute-done.4 = bf16[256,2048]{1,0:T(8,128)(2,1)S(1)} collective-permute-done((bf16[256,2048]{1,0:T(8,128)(2,1)}, bf16[256,2048]{1,0:T(8,128)(2,1)S(1)}, u32[]{:S(2)}, u32[]{:S(2)}) %collective-permute-start.4) | collective-permute-done | bytes 1048608 | tf_op jit(solution)/shard_map/ppermute | solution.py:24
  410.0 1.0 copy-done.11
  411.0 12.1 %convolution_convert_fusion = bf16[2048,1408]{1,0:T(8,128)(2,1)} fusion(bf16[1024,2048]{1,0:T(8,128)(2,1)} %constant_dynamic-update-slice_fusion, bf16[512,1408]{1,0:T(8,128)(2,1)} %collective-permute-done.1, bf16[512,1408]{1,0:T(8,128)(2,1)} %copy-done.9, bf16[512,1408]{1,0:T(8,128)(2,1)} %collective-permute-done.2, bf16[512,1408]{1,0:T(8,128)(2,1)} %get-tuple-element.14), kind=kOutput, calls=%fused_computation.4 | convolution fusion | flops 5928648704 | bytes 15728640 | tf_op jit(solution)/shard_map/dot_general | solution.py:12
  423.2 0.0 reduce-scatter.12.cloned.1.call-start
  423.3 3.1 constant_dynamic-update-slice_fusion.3
  426.4 3.4 constant_dynamic-update-slice_fusion.2
  429.8 10.9 %convolution_convert_fusion.1 = bf16[2048,1408]{1,0:T(8,128)(2,1)} fusion(bf16[1024,2048]{1,0:T(8,128)(2,1)} %constant_dynamic-update-slice_fusion.2, bf16[1024,1408]{1,0:T(8,128)(2,1)S(1)} %copy-done.16), kind=kOutput, calls=%fused_computation.5 | convolution fusion | flops 5908463616 | bytes 12845056 | tf_op jit(solution)/shard_map/dot_general | solution.py:12
  440.7 0.3 reduce-scatter.10.cloned.1.call-start
  441.0 1.6 copy-done.18
  442.5 10.9 %convolution_convert_fusion.2 = bf16[2048,1408]{1,0:T(8,128)(2,1)} fusion(bf16[1024,2048]{1,0:T(8,128)(2,1)} %constant_dynamic-update-slice_fusion.2, bf16[1024,1408]{1,0:T(8,128)(2,1)S(1)} %copy-done.18), kind=kOutput, calls=%fused_computation.6 | convolution fusion | flops 5908463616 | bytes 12845056 | tf_op jit(solution)/shard_map/dot_general | solution.py:12
  453.5 84.5 %reduce-scatter.14.cloned.1.call-done = bf16[256,1408]{1,0:T(8,128)(2,1)} async-done(((bf16[2048,1408]{1,0:T(8,128)(2,1)}), bf16[256,1408]{1,0:T(8,128)(2,1)}) %reduce-scatter.14.cloned.1.call-update) | async-done | bytes 720912 | tf_op jit(solution)/shard_map/reduce_scatter | solution.py:80
  537.9 1.5 collective-permute-start.7
  539.4 1.8 broadcast.66.clone.2
  541.2 1.2 convert_dynamic-update-slice_fusion.1
  542.4 13.0 %collective-permute-done.7 = bf16[256,1408]{1,0:T(8,128)(2,1)S(1)} collective-permute-done((bf16[256,1408]{1,0:T(8,128)(2,1)}, bf16[256,1408]{1,0:T(8,128)(2,1)S(1)}, u32[]{:S(2)}, u32[]{:S(2)}) %collective-permute-start.7) | collective-permute-done | bytes 720928 | tf_op jit(solution)/shard_map/ppermute | solution.py:24
  555.3 1.2 convert_dynamic-update-slice_fusion
  556.5 95.0 %reduce-scatter.12.cloned.1.call-done = bf16[256,1408]{1,0:T(8,128)(2,1)} async-done(((bf16[2048,1408]{1,0:T(8,128)(2,1)}), bf16[256,1408]{1,0:T(8,128)(2,1)}) %reduce-scatter.12.cloned.1.call-update) | async-done | bytes 720912 | tf_op jit(solution)/shard_map/reduce_scatter | solution.py:80
  651.5 1.5 collective-permute-start.6
  653.0 1.8 broadcast.66.clone.1
  654.8 1.2 convert_dynamic-update-slice_fusion.3
  656.0 109.1 %reduce-scatter.10.cloned.1.call-done = bf16[256,1408]{1,0:T(8,128)(2,1)} async-done(((bf16[2048,1408]{1,0:T(8,128)(2,1)}), bf16[256,1408]{1,0:T(8,128)(2,1)}) %reduce-scatter.10.cloned.1.call-update) | async-done | bytes 720912 | tf_op jit(solution)/shard_map/reduce_scatter | solution.py:80
  765.1 1.5 collective-permute-start.5
  766.5 0.2 broadcast.66.clone
  766.7 0.1 convert_dynamic-update-slice_fusion.5
  766.8 1.2 convert_dynamic-update-slice_fusion.2
  768.0 14.4 %collective-permute-done.5 = bf16[256,1408]{1,0:T(8,128)(2,1)S(1)} collective-permute-done((bf16[256,1408]{1,0:T(8,128)(2,1)}, bf16[256,1408]{1,0:T(8,128)(2,1)S(1)}, u32[]{:S(2)}, u32[]{:S(2)}) %collective-permute-start.5) | collective-permute-done | bytes 720928 | tf_op jit(solution)/shard_map/ppermute | solution.py:24
  782.4 0.1 convert_dynamic-update-slice_fusion.4
  782.5 1.6 copy-done.7
  (59 shorter events, 0.5 us)
Async XLA Ops:
  7.2 33.6 %copy-start = (bf16[256,2816]{1,0:T(8,128)(2,1)S(1)}, bf16[256,2816]{1,0:T(8,128)(2,1)}, u32[]{:S(2)}) copy-start(bf16[256,2816]{1,0:T(8,128)(2,1)} %param.19) | copy-start | bytes 4325380
  7.2 45.2 %all-gather.8.cloned.1.call-start = ((), (), s32[]{:S(2)}) async-start(), calls=%async_computation.5 | async-start | bytes 3145728 | tf_op jit(solution)/shard_map/all_gather | solution.py:69
  13.3 42.3 %all-gather.10.cloned.1.call-start = ((), (), s32[]{:S(2)}) async-start(), calls=%async_computation.6 | async-start | bytes 3145728 | tf_op jit(solution)/shard_map/all_gather | solution.py:69
  13.3 26.4 %collective-permute-start = (bf16[256,2048]{1,0:T(8,128)(2,1)}, bf16[256,2048]{1,0:T(8,128)(2,1)S(1)}, u32[]{:S(2)}, u32[]{:S(2)}) collective-permute-start(bf16[256,2048]{1,0:T(8,128)(2,1)} %fusion.11), channel_id=1, source_target_pairs={{0,16},{16,0},{1,17},{17,1},{2,18},{18,2},{3,19},{19,3},{4,20},{20... | collective-permute-start | bytes 3145736 | tf_op jit(solution)/shard_map/ppermute | solution.py:24
  39.7 1.0 copy-start.10
  40.7 107.9 %all-gather.12.cloned.1.call-start = ((), (), s32[]{:S(2)}) async-start(), calls=%async_computation.7 | async-start | bytes 6488064 | tf_op jit(solution)/shard_map/all_gather | solution.py:47
  41.7 4.5 copy-start.5
  41.7 199.5 %all-gather.16.cloned.1.call-start = ((), (), s32[]{:S(2)}) async-start(), calls=%async_computation.9 | async-start | bytes 6488064 | tf_op jit(solution)/shard_map/all_gather | solution.py:99
  44.0 289.7 %all-gather.14.cloned.1.call-start = ((), (), s32[]{:S(2)}) async-start(), calls=%async_computation.8 | async-start | bytes 6488064 | tf_op jit(solution)/shard_map/all_gather | solution.py:98
  46.1 309.0 %reduce-scatter.8.cloned.1.call-start = ((), (), s32[]{:S(2)}) async-start(), calls=%async_computation.11 | async-start | bytes 3145728 | tf_op jit(solution)/shard_map/reduce_scatter | solution.py:104
  46.2 3.7 copy-start.6
  48.0 34.8 %collective-permute-start.2 = (bf16[512,1408]{1,0:T(8,128)(2,1)}, bf16[512,1408]{1,0:T(8,128)(2,1)}, u32[]{:S(2)}, u32[]{:S(2)}) collective-permute-start(bf16[512,1408]{1,0:T(8,128)(2,1)} %get-tuple-element.15), channel_id=1, source_target_pairs={{0,16},{16,0},{1,17},{17,1},{2,18},{18,2},{3,19},{19,3},{4,20},{20... | collective-permute-start | bytes 4325384 | tf_op jit(solution)/shard_map/ppermute | solution.py:24
  51.3 97.4 %copy-start.9 = (bf16[512,1408]{1,0:T(8,128)(2,1)}, bf16[512,1408]{1,0:T(8,128)(2,1)S(1)}, u32[]{:S(2)}) copy-start(bf16[512,1408]{1,0:T(8,128)(2,1)S(1)} %get-tuple-element.12) | copy-start | bytes 4325380
  51.3 60.7 %collective-permute-start.1 = (bf16[512,1408]{1,0:T(8,128)(2,1)}, bf16[512,1408]{1,0:T(8,128)(2,1)}, u32[]{:S(2)}, u32[]{:S(2)}) collective-permute-start(bf16[512,1408]{1,0:T(8,128)(2,1)} %get-tuple-element.13), channel_id=1, source_target_pairs={{0,16},{16,0},{1,17},{17,1},{2,18},{18,2},{3,19},{19,3},{4,20},{20... | collective-permute-start | bytes 4325384 | tf_op jit(solution)/shard_map/ppermute | solution.py:24
  55.5 93.1 %copy-start.8 = (bf16[512,1408]{1,0:T(8,128)(2,1)S(1)}, bf16[512,1408]{1,0:T(8,128)(2,1)}, u32[]{:S(2)}) copy-start(bf16[512,1408]{1,0:T(8,128)(2,1)} %get-tuple-element.14) | copy-start | bytes 4325380
  241.2 92.6 %copy-start.17 = (bf16[1024,1408]{1,0:T(8,128)(2,1)S(1)}, bf16[1024,1408]{1,0:T(8,128)(2,1)}, u32[]{:S(2)}) copy-start(bf16[1024,1408]{1,0:T(8,128)(2,1)} %get-tuple-element.8) | copy-start | bytes 8650756
  347.0 33.7 %copy-start.3 = (bf16[256,2048]{1,0:T(8,128)(2,1)S(1)}, bf16[256,2048]{1,0:T(8,128)(2,1)}, u32[]{:S(2)}) copy-start(bf16[256,2048]{1,0:T(8,128)(2,1)} %param.10) | copy-start | bytes 3145732
  347.0 33.7 %copy-start.15 = (f32[2048]{0:T(1024)S(1)}, f32[2048]{0:T(1024)}, u32[]{:S(2)}) copy-start(f32[2048]{0:T(1024)} %param.11) | copy-start | bytes 24580
  347.1 35.6 %copy-start.2 = (bf16[256,2048]{1,0:T(8,128)(2,1)S(1)}, bf16[256,2048]{1,0:T(8,128)(2,1)}, u32[]{:S(2)}) copy-start(bf16[256,2048]{1,0:T(8,128)(2,1)} %param.16) | copy-start | bytes 3145732
  347.1 21.9 %reduce-scatter.6.cloned.1.call-start = ((), (), s32[]{:S(2)}) async-start(), calls=%async_computation.10 | async-start | bytes 3145728 | tf_op jit(solution)/shard_map/reduce_scatter | solution.py:104
  347.8 75.4 %all-gather.18.cloned.1.call-start = ((), (), s32[]{:S(2)}) async-start(), calls=%async_computation.12 | async-start | bytes 3145728 | tf_op jit(solution)/shard_map/all_gather | solution.py:68
  355.2 25.6 %collective-permute-start.3 = (bf16[256,2048]{1,0:T(8,128)(2,1)}, bf16[256,2048]{1,0:T(8,128)(2,1)S(1)}, u32[]{:S(2)}, u32[]{:S(2)}) collective-permute-start(bf16[256,2048]{1,0:T(8,128)(2,1)} %reduce-scatter.8.cloned.1.call-done), channel_id=1, source_target_pairs={{0,16},{16,0},{1,17},{17,1},{2,18},{18,2},{3,19},{19,3},{4,20},{20... | collective-permute-start | bytes 3145736 | tf_op jit(solution)/shard_map/ppermute | solution.py:24
  369.0 13.7 %copy-start.4 = (bf16[256,2048]{1,0:T(8,128)(2,1)S(1)}, bf16[256,2048]{1,0:T(8,128)(2,1)}, u32[]{:S(2)}) copy-start(bf16[256,2048]{1,0:T(8,128)(2,1)} %reduce-scatter.6.cloned.1.call-done) | copy-start | bytes 3145732
  385.1 41.3 %all-gather.20.cloned.1.call-start = ((), (), s32[]{:S(2)}) async-start(), calls=%async_computation.13 | async-start | bytes 3145728 | tf_op jit(solution)/shard_map/all_gather | solution.py:68
  385.2 24.8 %collective-permute-start.4 = (bf16[256,2048]{1,0:T(8,128)(2,1)}, bf16[256,2048]{1,0:T(8,128)(2,1)S(1)}, u32[]{:S(2)}, u32[]{:S(2)}) collective-permute-start(bf16[256,2048]{1,0:T(8,128)(2,1)} %get-tuple-element.16), channel_id=1, source_target_pairs={{0,16},{16,0},{1,17},{17,1},{2,18},{18,2},{3,19},{19,3},{4,20},{20... | collective-permute-start | bytes 3145736 | tf_op jit(solution)/shard_map/ppermute | solution.py:24
  410.0 1.0 copy-start.11
  411.0 127.0 %reduce-scatter.14.cloned.1.call-start = ((), (), s32[]{:S(2)}) async-start(), calls=%async_computation.16 | async-start | bytes 6488064 | tf_op jit(solution)/shard_map/reduce_scatter | solution.py:80
  423.2 228.4 %reduce-scatter.12.cloned.1.call-start = ((), (), s32[]{:S(2)}) async-start(), calls=%async_computation.15 | async-start | bytes 6488064 | tf_op jit(solution)/shard_map/reduce_scatter | solution.py:80
  426.4 3.4 copy-start.16
  440.7 1.9 copy-start.18
  440.7 324.3 %reduce-scatter.10.cloned.1.call-start = ((), (), s32[]{:S(2)}) async-start(), calls=%async_computation.14 | async-start | bytes 6488064 | tf_op jit(solution)/shard_map/reduce_scatter | solution.py:80
  537.9 3.2 copy-start.13
  537.9 17.4 %collective-permute-start.7 = (bf16[256,1408]{1,0:T(8,128)(2,1)}, bf16[256,1408]{1,0:T(8,128)(2,1)S(1)}, u32[]{:S(2)}, u32[]{:S(2)}) collective-permute-start(bf16[256,1408]{1,0:T(8,128)(2,1)} %reduce-scatter.14.cloned.1.call-done), channel_id=1, source_target_pairs={{0,16},{16,0},{1,17},{17,1},{2,18},{18,2},{3,19},{19,3},{4,20},{20... | collective-permute-start | bytes 2162696 | tf_op jit(solution)/shard_map/ppermute | solution.py:24
  651.5 3.3 copy-start.12
  651.5 115.3 %collective-permute-start.6 = (bf16[256,1408]{1,0:T(8,128)(2,1)}, bf16[256,1408]{1,0:T(8,128)(2,1)S(1)}, u32[]{:S(2)}, u32[]{:S(2)}) collective-permute-start(bf16[256,1408]{1,0:T(8,128)(2,1)} %reduce-scatter.12.cloned.1.call-done), channel_id=1, source_target_pairs={{0,16},{16,0},{1,17},{17,1},{2,18},{18,2},{3,19},{19,3},{4,20},{20... | collective-permute-start | bytes 2162696 | tf_op jit(solution)/shard_map/ppermute | solution.py:24
  765.0 1.7 copy-start.14
  765.1 17.4 %collective-permute-start.5 = (bf16[256,1408]{1,0:T(8,128)(2,1)}, bf16[256,1408]{1,0:T(8,128)(2,1)S(1)}, u32[]{:S(2)}, u32[]{:S(2)}) collective-permute-start(bf16[256,1408]{1,0:T(8,128)(2,1)} %reduce-scatter.10.cloned.1.call-done), channel_id=1, source_target_pairs={{0,16},{16,0},{1,17},{17,1},{2,18},{18,2},{3,19},{19,3},{4,20},{20... | collective-permute-start | bytes 2162696 | tf_op jit(solution)/shard_map/ppermute | solution.py:24
  766.5 17.6 %copy-start.1 = (bf16[256,2816]{1,0:T(8,128)(2,1)S(1)}, bf16[256,2816]{1,0:T(8,128)(2,1)}, u32[]{:S(2)}) copy-start(bf16[256,2816]{1,0:T(8,128)(2,1)} %param.19) | copy-start | bytes 4325380
  782.5 1.6 copy-start.7
Sparse Core Ops, SparseCore 0:
  13.4 13.2 all-gather.7
  40.8 12.0 all-gather.9
  55.1 93.4 all-gather.11
  150.7 90.4 all-gather.15
  243.2 90.4 all-gather.13
  347.2 7.9 reduce-scatter.7
  358.0 11.0 reduce-scatter.5
  385.2 11.6 all-gather.17
  411.1 11.4 all-gather.19
  426.1 111.7 reduce-scatter.13
  541.6 109.9 reduce-scatter.11
  655.0 109.9 reduce-scatter.9
